TPU v7x, 32 devices: a whole 2x2x4 slice. The times are simulated.
32 devices in a mesh: sp: 8 (over z, y), dp: 4 (over x, core).
Axes of the slice: x: 2, y: 2, z: 4, core: 2. Of those that a mesh axis runs over, the one named last changes fastest.
Arguments:
- query_nope: bfloat16 [4, 2048, 16, 128], P('dp', 'sp'), may hold values from -6 to 6
- query_rope: bfloat16 [4, 2048, 16, 64], P('dp', 'sp'), may hold values from -160 to 160
- latent: bfloat16 [4, 2048, 256], P('dp', 'sp'), may hold values from -6 to 6
- key_rope: bfloat16 [4, 2048, 64], P('dp', 'sp'), may hold values from -4 to 4
- resid: bfloat16 [4, 2048, 2048], P('dp', 'sp'), may hold values from -6 to 6
- latent_gain: float32 [256], replicated, may hold values from 0.1 to 1.9
- key_up: bfloat16 [256, 2048], P(None, 'sp'), may hold values from -0.375 to 0.375
- value_up: bfloat16 [256, 2048], P(None, 'sp'), may hold values from -0.375 to 0.375
- out_proj: bfloat16 [2048, 2048], P('sp', 'dp'), may hold values from -0.125 to 0.125
- norm_gain: float32 [2048], replicated, may hold values from 0.1 to 1.9
- expert_gate: bfloat16 [8, 2048, 1024], P('sp'), may hold values from -0.125 to 0.125
- expert_up: bfloat16 [8, 2048, 1024], P('sp'), may hold values from -0.125 to 0.125
- expert_down: bfloat16 [8, 1024, 2048], P('sp'), may hold values from -0.1875 to 0.1875
- routes: int32 [4, 2048, 2], P('dp', 'sp'), may hold values from 0 to 7, all different within a row; in each aligned block of 256 rows (0 to 255, 256 to 511, ..., all dimensions but the last counted through in order) at most 128 rows name the same one
- route_weight: float32 [4, 2048, 2], P('dp', 'sp'), may hold values from 0.2 to 1
Outputs:
- mixed: bfloat16 [4, 2048, 2048], P('dp', 'sp')
Inputs may be any that keep to these rules, and one draw needn't show every extreme that they name: `routes`: each token names two different experts. Among the tokens of one device no expert is named more than 128 times, and in every draw some expert is named exactly 128 times by some device's tokens.
All inputs are finite; a program needn't handle non-finite values.
Results may differ from a plain program's by a relative error of at most 0.0075.
Values may be sent and summed in bfloat16 or wider, within the bound.
No kernel may reach another device: no remote copies, remote signals or barrier semaphores. Data moves between devices by JAX's collectives and lax.ppermute only.
A program may use at most 128 MiB of HBM per device.

v0:
```python
import jax
import jax.numpy as jnp
from jax import lax
from jax.sharding import PartitionSpec as P

epsilon = 1e-06
rope_base = 10000.0
masked_score = -1e30


def rotate(values, positions):
    half_width = values.shape[-1] // 2
    frequency = rope_base ** (-jnp.arange(half_width, dtype=jnp.float32) / half_width)
    angles = positions.astype(jnp.float32)[:, None] * frequency[None, :]
    cosine = jnp.cos(angles)
    sine_part = jnp.sin(angles)
    if values.ndim == 3:
        cosine = cosine[:, None, :]
        sine_part = sine_part[:, None, :]
    floats = values.astype(jnp.float32)
    first_half = floats[..., :half_width]
    second_half = floats[..., half_width:]
    turned = jnp.concatenate(
        [
            first_half * cosine - second_half * sine_part,
            second_half * cosine + first_half * sine_part,
        ],
        axis=-1,
    )
    return turned.astype(jnp.bfloat16)


def rms_scaled(values, gain):
    floats = values.astype(jnp.float32)
    return floats * lax.rsqrt(jnp.mean(floats * floats, axis=-1, keepdims=True) + epsilon) * gain


def assign_slots(route_block, experts_all, capacity):
    flat_routes = route_block.reshape(-1)
    onehot = (flat_routes[:, None] == jnp.arange(experts_all, dtype=jnp.int32)[None, :]).astype(
        jnp.int32
    )
    earlier = jnp.cumsum(onehot, axis=0) - onehot
    placed = jnp.sum(earlier * onehot, axis=1)
    return flat_routes * capacity + placed


def fill_slots(rows, slot_ids, experts_all, capacity):
    pairs = slot_ids.shape[0]
    matches = jnp.arange(experts_all * capacity, dtype=jnp.int32)[:, None] == slot_ids[None, :]
    source = (
        jnp.sum(jnp.where(matches, jnp.arange(pairs, dtype=jnp.int32)[None, :], 0), axis=1) // 2
    )
    filled = jnp.any(matches, axis=1)
    picked = jnp.take(rows, source, axis=0)
    chosen = jnp.where(filled[:, None], picked, jnp.zeros_like(picked))
    return chosen.reshape(experts_all, capacity, rows.shape[-1])


def combine_slots(returned, slot_ids, weights):
    flat_back = returned.reshape(-1, returned.shape[-1])
    picked = (
        jnp.take(flat_back, slot_ids, axis=0).astype(jnp.float32).reshape(weights.shape[0], 2, -1)
    )
    return jnp.sum(weights[:, :, None] * picked, axis=1)


def shards(
    query_nope,
    query_rope,
    latent,
    key_rope,
    resid,
    latent_gain,
    key_up,
    value_up,
    out_proj,
    norm_gain,
    expert_gate,
    expert_up,
    expert_down,
    routes,
    route_weight,
):
    tokens_here = latent.shape[1]
    sp_count = lax.axis_size("sp")
    length = tokens_here * sp_count
    block = min(512, length)
    blocks = length // block
    local_pos = lax.axis_index("sp") * tokens_here + jnp.arange(tokens_here, dtype=jnp.int32)
    latent_normed = rms_scaled(latent[0], latent_gain).astype(jnp.bfloat16)
    key_turned = rotate(key_rope[0], local_pos)
    query_turned = rotate(query_rope[0], local_pos)
    all_latent, all_keyturn = (
        lax.all_gather(latent_normed, "sp", axis=0, tiled=True),
        lax.all_gather(key_turned, "sp", axis=0, tiled=True),
    )
    query_plain, query_turn = (
        lax.all_to_all(query_nope[0], "sp", split_axis=1, concat_axis=0, tiled=True),
        lax.all_to_all(query_turned, "sp", split_axis=1, concat_axis=0, tiled=True),
    )
    heads_here = query_plain.shape[1]
    key_plain = (
        jnp.dot(all_latent, key_up, preferred_element_type=jnp.float32)
        .astype(jnp.bfloat16)
        .reshape(length, heads_here, -1)
    )
    value_heads = (
        jnp.dot(all_latent, value_up, preferred_element_type=jnp.float32)
        .astype(jnp.bfloat16)
        .reshape(length, heads_here, -1)
    )
    scale = (query_plain.shape[-1] + query_turn.shape[-1]) ** (-0.5)
    key_ids = jnp.arange(length, dtype=jnp.int32)

    def one_block(items):
        index, plain_block, turn_block = items
        scores = jnp.einsum(
            "bhd,shd->hbs", plain_block, key_plain, preferred_element_type=jnp.float32
        )
        scores = (
            scores
            + jnp.einsum("bhr,sr->hbs", turn_block, all_keyturn, preferred_element_type=jnp.float32)
        ) * scale
        row_ids = index * block + jnp.arange(block, dtype=jnp.int32)
        allowed = key_ids[None, :] <= row_ids[:, None]
        scores = jnp.where(allowed[None], scores, masked_score)
        largest = jnp.max(scores, axis=-1, keepdims=True)
        powers = jnp.exp(scores - largest)
        attend = (powers / jnp.sum(powers, axis=-1, keepdims=True)).astype(jnp.bfloat16)
        return jnp.einsum(
            "hbs,shd->bhd", attend, value_heads, preferred_element_type=jnp.float32
        ).astype(jnp.bfloat16)

    attended = lax.map(
        one_block,
        (
            jnp.arange(blocks, dtype=jnp.int32),
            query_plain.reshape(blocks, block, heads_here, -1),
            query_turn.reshape(blocks, block, heads_here, -1),
        ),
    )
    attended = attended.reshape(length, heads_here, -1)
    token_heads = lax.all_to_all(attended, "sp", split_axis=0, concat_axis=1, tiled=True)
    flat_heads = token_heads.reshape(tokens_here, -1)
    head_rows = lax.all_gather(out_proj, "dp", axis=1, tiled=True)
    projected = jnp.dot(
        flat_heads,
        lax.all_gather(head_rows, "sp", axis=0, tiled=True),
        preferred_element_type=jnp.float32,
    ).astype(jnp.bfloat16)
    after_attention = resid[0].astype(jnp.float32) + projected.astype(jnp.float32)
    normed = rms_scaled(after_attention, norm_gain).astype(jnp.bfloat16)
    experts_all = sp_count * expert_gate.shape[0]
    capacity = 4 * tokens_here // experts_all
    slot_ids = assign_slots(routes[0], experts_all, capacity)
    outgoing = fill_slots(normed, slot_ids, experts_all, capacity)
    arrived = lax.all_to_all(outgoing, "sp", split_axis=0, concat_axis=0, tiled=True)
    senders, slots_now, width = arrived.shape
    rows = arrived.reshape(senders * slots_now, width)
    gate = jnp.dot(rows, expert_gate[0], preferred_element_type=jnp.float32)
    upward = jnp.dot(rows, expert_up[0], preferred_element_type=jnp.float32)
    hidden = (jax.nn.silu(gate) * upward).astype(jnp.bfloat16)
    result = jnp.dot(hidden, expert_down[0], preferred_element_type=jnp.float32).astype(
        jnp.bfloat16
    )
    returned = lax.all_to_all(
        result.reshape(senders, slots_now, width), "sp", split_axis=0, concat_axis=0, tiled=True
    )
    routed = combine_slots(returned, slot_ids, route_weight[0])
    return (after_attention + routed).astype(jnp.bfloat16)[None]


def solution(mesh):
    return jax.shard_map(
        shards,
        mesh=mesh,
        in_specs=(
            P("dp", "sp", None, None),
            P("dp", "sp", None, None),
            P("dp", "sp", None),
            P("dp", "sp", None),
            P("dp", "sp", None),
            P(),
            P(None, "sp"),
            P(None, "sp"),
            P("sp", "dp"),
            P(),
            P("sp", None, None),
            P("sp", None, None),
            P("sp", None, None),
            P("dp", "sp", None),
            P("dp", "sp", None),
        ),
        out_specs=P("dp", "sp", None),
        check_vma=False,
    )
```

profile of v0, /device:TPU:0, one launch (start us, length us, event | category | flops | bytes accessed | tf_op | source)
XLA Modules:
  0.0 489.6 jit_solution(9054582442500225814)
XLA Ops:
  8.3 1.7 fusion.35
  12.2 16.1 %all-gather.6.cloned.1.call-done = bf16[256,2048]{1,0:T(8,128)(2,1)} async-done(((bf16[256,512]{1,0:T(8,128)(2,1)}), bf16[256,2048]{1,0:T(8,128)(2,1)}) %all-gather.6.cloned.1.call-update) | async-done | bytes 1048592 | tf_op jit(solution)/shard_map/all_gather | solution.py:146
  29.4 5.5 %all-to-all-start.1 = ((bf16[256,16,64]{0,2,1:T(8,128)(2,1)}), bf16[256,16,64]{0,2,1:T(8,128)(2,1)S(1)}, u32[]{:S(2)}, u32[]{:S(2)}) async-start(bf16[256,16,64]{0,2,1:T(8,128)(2,1)} %pad_maximum_fusion), calls=%async_computation.1 | async-start | bytes 1048576 | tf_op jit(solution)/shard_map/all_to_all | solution.py:100
  34.9 1.3 copy.109
  36.2 17.7 %all-to-all-done.1 = bf16[256,16,64]{0,2,1:T(8,128)(2,1)S(1)} async-done(((bf16[256,16,64]{0,2,1:T(8,128)(2,1)}), bf16[256,16,64]{0,2,1:T(8,128)(2,1)S(1)}, u32[]{:S(2)}, u32[]{:S(2)}) %all-to-all-start.1) | async-done | bytes 524320 | tf_op jit(solution)/shard_map/all_to_all | solution.py:100
  54.0 3.6 all-to-all-start
  57.6 55.9 %all_gather.13 = bf16[2048,64]{0,1:T(8,128)(2,1)S(1)} all-gather(bf16[256,64]{0,1:T(8,128)(2,1)S(1)} %pad_maximum_fusion.1), channel_id=1, replica_groups=mesh['sp'=8,'dp'=4] {'sp'}, dimensions={0}, use_global_device_ids=true | all-gather | bytes 294912 | tf_op jit(solution)/shard_map/all_gather | solution.py:96
  115.1 2.8 convolution_convert_fusion.1
  117.9 1.6 copy.91
  119.5 2.4 convolution_convert_fusion
  121.9 2.3 copy.93
  124.3 73.1 %while.11 = (s32[]{:T(128)}, bf16[4,512,2,128]{3,1,0,2:T(8,128)(2,1)}, s32[4]{0:T(128)S(1)}, bf16[4,512,2,128]{3,1,0,2:T(8,128)(2,1)S(1)}, bf16[2048,2,128]{2,0,...) while((s32[]{:T(128)}, ...), condition=%wide.region_4.5_spmd.clone, body=%wide.region_1.4_spmd.clone.sunk | while | flops 1360139776 | bytes 93205688 | solution.py:135
  124.3 1.3 fusion.74
  127.3 2.8 fusion.75
  130.1 1.5 fusion.76
  131.7 1.6 copy-done.2
  133.3 9.1 %fusion.77 = bf16[4,512,2,128]{3,1,0,2:T(8,128)(2,1)} fusion(bf16[4,512,2,128]{3,1,0,2:T(8,128)(2,1)} %get-tuple-element.211, s32[]{:T(128)} %get-tuple-element.210, bf16[2048,2,128]{2,0,1:T(8,128)(2,1)S(1)} %copy-done.5, f32[2,512]{1,0:T(2,128)S(1)} %fusion.76, f32[2,512,2048]{2,1,0:T(8,128)} %copy-done.2), kind=kOutput, calls=%fused_computation.13.clone.1 | convolution fusion | flops 543296512 | bytes 18092544 | tf_op jit(solution)/shard_map/while/body/eval_jaxpr/hbs,shd->bhd/dot_general | solution.py:131
  142.4 1.2 fusion.74
  145.5 2.8 fusion.75
  148.3 1.5 fusion.76
  149.9 1.6 copy-done.2
  151.5 9.2 %fusion.77 = bf16[4,512,2,128]{3,1,0,2:T(8,128)(2,1)} fusion(bf16[4,512,2,128]{3,1,0,2:T(8,128)(2,1)} %get-tuple-element.211, s32[]{:T(128)} %get-tuple-element.210, bf16[2048,2,128]{2,0,1:T(8,128)(2,1)S(1)} %copy-done.5, f32[2,512]{1,0:T(2,128)S(1)} %fusion.76, f32[2,512,2048]{2,1,0:T(8,128)} %copy-done.2), kind=kOutput, calls=%fused_computation.13.clone.1 | convolution fusion | flops 543296512 | bytes 18092544 | tf_op jit(solution)/shard_map/while/body/eval_jaxpr/hbs,shd->bhd/dot_general | solution.py:131
  160.7 1.2 fusion.74
  163.8 2.8 fusion.75
  166.6 1.5 fusion.76
  168.1 1.6 copy-done.2
  169.8 9.1 %fusion.77 = bf16[4,512,2,128]{3,1,0,2:T(8,128)(2,1)} fusion(bf16[4,512,2,128]{3,1,0,2:T(8,128)(2,1)} %get-tuple-element.211, s32[]{:T(128)} %get-tuple-element.210, bf16[2048,2,128]{2,0,1:T(8,128)(2,1)S(1)} %copy-done.5, f32[2,512]{1,0:T(2,128)S(1)} %fusion.76, f32[2,512,2048]{2,1,0:T(8,128)} %copy-done.2), kind=kOutput, calls=%fused_computation.13.clone.1 | convolution fusion | flops 543296512 | bytes 18092544 | tf_op jit(solution)/shard_map/while/body/eval_jaxpr/hbs,shd->bhd/dot_general | solution.py:131
  178.9 1.2 fusion.74
  181.9 2.8 fusion.75
  184.7 1.5 fusion.76
  186.3 1.7 copy-done.2
  188.0 9.4 %fusion.77 = bf16[4,512,2,128]{3,1,0,2:T(8,128)(2,1)} fusion(bf16[4,512,2,128]{3,1,0,2:T(8,128)(2,1)} %get-tuple-element.211, s32[]{:T(128)} %get-tuple-element.210, bf16[2048,2,128]{2,0,1:T(8,128)(2,1)S(1)} %copy-done.5, f32[2,512]{1,0:T(2,128)S(1)} %fusion.76, f32[2,512,2048]{2,1,0:T(8,128)} %copy-done.2), kind=kOutput, calls=%fused_computation.13.clone.1 | convolution fusion | flops 543296512 | bytes 18092544 | tf_op jit(solution)/shard_map/while/body/eval_jaxpr/hbs,shd->bhd/dot_general | solution.py:131
  197.3 3.7 copy.95
  201.0 3.7 all-to-all-start.2
  207.4 28.0 %all-to-all-done.2 = bf16[2048,2,128]{2,1,0:T(2,128)(2,1)S(1)} async-done(((bf16[2048,2,128]{2,1,0:T(2,128)(2,1)}), bf16[2048,2,128]{2,1,0:T(2,128)(2,1)S(1)}, u32[]{:S(2)}, u32[]{:S(2)}) %all-to-all-start.2) | async-done | bytes 1048608 | tf_op jit(solution)/shard_map/all_to_all | solution.py:144
  236.2 6.1 %multiply_reduce_fusion.1 = (f32[256]{0:T(256)S(1)}, f32[256,2048]{1,0:T(8,128)S(1)}) fusion(bf16[256,2048]{0,1:T(8,128)(2,1)S(1)} %bitcast.150, bf16[2048,2048]{1,0:T(8,128)(2,1)} %all-gather.8.cloned.1.call-done, bf16[1,256,2048]{2,1,0:T(8,128)(2,1)} %param.21), kind=kOutput, calls=%fused_computation.42 | convolution fusion | flops 2150629120 | bytes 12583936 | tf_op jit(solution)/shard_map/dot_general | solution.py:147
  242.5 6.0 %gather_fusion = bf16[1024,2048]{1,0:T(8,128)(2,1)} fusion(bf16[256,2048]{1,0:T(8,128)(2,1)S(1)} %multiply_convert_fusion.1, s32[1024]{0:T(1024)S(1)} %broadcast_clamp_fusion), kind=kCustom, calls=%fused_computation | custom fusion | bytes 8392704 | tf_op jit(solution)/shard_map/jit(_take)/gather | solution.py:55
  248.5 2.6 select_select_fusion
  251.1 95.5 %all_to_all.55 = bf16[8,128,2048]{2,1,0:T(8,128)(2,1)S(1)} all-to-all(bf16[8,128,2048]{2,1,0:T(8,128)(2,1)S(1)} %select_select_fusion), channel_id=1, replica_groups=mesh['sp'=8,'dp'=4] {'sp'}, dimensions={0} | all-to-all | bytes 8388608 | tf_op jit(solution)/shard_map/all_to_all | solution.py:158
  346.6 4.5 fusion.20
  351.1 5.4 %multiply_convert_fusion = bf16[1024,1024]{1,0:T(8,128)(2,1)S(1)} fusion(f32[1024,1024]{1,0:T(8,128)S(1)} %fusion.20, bf16[1024,2048]{1,0:T(8,128)(2,1)S(1)} %bitcast.154, bf16[1,2048,1024]{2,1,0:T(8,128)(2,1)S(1)} %copy-done.10), kind=kOutput, calls=%fused_computation.31 | convolution fusion | flops 4301258752 | bytes 14680064 | tf_op jit(solution)/shard_map/dot_general | solution.py:161
  356.5 6.1 %fusion.24 = bf16[1024,2048]{1,0:T(8,128)(2,1)} fusion(bf16[1024,1024]{1,0:T(8,128)(2,1)S(1)} %multiply_convert_fusion, bf16[1,1024,2048]{2,1,0:T(8,128)(2,1)S(1)} %copy-done.11), kind=kOutput, calls=%fused_computation.34 | convolution fusion | flops 4297064448 | bytes 10485760 | tf_op jit(solution)/shard_map/dot_general | solution.py:164
  362.6 4.9 all-to-all-start.4
  368.4 91.0 %all-to-all-done.4 = bf16[8,128,2048]{2,1,0:T(8,128)(2,1)} async-done(((bf16[8,128,2048]{2,1,0:T(8,128)(2,1)}), bf16[8,128,2048]{2,1,0:T(8,128)(2,1)}, u32[]{:S(2)}, u32[]{:S(2)}) %all-to-all-start.4) | async-done | bytes 4194336 | tf_op jit(solution)/shard_map/all_to_all | solution.py:167
  459.4 8.0 %gather_fusion.1 = bf16[512,2048]{1,0:T(8,128)(2,1)} fusion(bf16[1024,2048]{1,0:T(8,128)(2,1)} %bitcast.33, s32[1024]{0:T(1024)S(1)} %pad_clamp_fusion), kind=kCustom, calls=%fused_computation.1 | custom fusion | bytes 4196352 | tf_op jit(solution)/shard_map/jit(_take)/gather | solution.py:63
  467.4 4.4 gather.15
  471.9 9.9 %multiply_reduce_fusion = f32[256,2048]{1,0:T(8,128)S(1)} fusion(bf16[256,2,2048]{2,1,0:T(2,128)(2,1)} %gather.15, pred[256,2]{1,0:T(8,128)(4,1)S(1)} %copy.102, f32[256,2]{1,0:T(8,128)S(1)} %copy.98), kind=kLoop, calls=%fused_computation.30 | loop fusion | flops 3670016 | bytes 4196864 | tf_op jit(solution)/shard_map/reduce_sum | solution.py:65
  481.8 1.3 fusion.32
  (98 shorter events, 15.8 us)
Async XLA Ops:
  6.5 108.5 %copy-start = (bf16[256,256]{1,0:T(8,128)(2,1)S(1)}, bf16[256,256]{1,0:T(8,128)(2,1)}, u32[]{:S(2)}) copy-start(bf16[256,256]{1,0:T(8,128)(2,1)} %param.23) | copy-start | bytes 393220
  6.5 28.3 %copy-start.4 = (bf16[1,256,16,128]{3,2,1,0:T(8,128)(2,1)S(1)}, bf16[1,256,16,128]{3,2,1,0:T(8,128)(2,1)}, u32[]{:S(2)}) copy-start(bf16[1,256,16,128]{3,2,1,0:T(8,128)(2,1)} %param.17) | copy-start | bytes 3145732
  6.5 21.8 %all-gather.6.cloned.1.call-start = ((), (), s32[]{:S(2)}) async-start(), calls=%async_computation.6 | async-start | bytes 1310720 | tf_op jit(solution)/shard_map/all_gather | solution.py:146
  7.3 107.8 %all-gather.4.cloned.1.call-start = ((), (), s32[]{:S(2)}) async-start(), calls=%async_computation.5 | async-start | bytes 1179648 | tf_op jit(solution)/shard_map/all_gather | solution.py:95
  10.0 226.1 %all-gather.8.cloned.1.call-start = ((), (), s32[]{:S(2)}) async-start(), calls=%async_computation.7 | async-start | bytes 9437184 | tf_op jit(solution)/shard_map/all_gather | solution.py:149
  29.4 24.6 %all-to-all-start.1 = ((bf16[256,16,64]{0,2,1:T(8,128)(2,1)}), bf16[256,16,64]{0,2,1:T(8,128)(2,1)S(1)}, u32[]{:S(2)}, u32[]{:S(2)}) async-start(bf16[256,16,64]{0,2,1:T(8,128)(2,1)} %pad_maximum_fusion), calls=%async_computation.1 | async-start | bytes 1048576 | tf_op jit(solution)/shard_map/all_to_all | solution.py:100
  54.0 70.2 %all-to-all-start = ((bf16[256,16,128]{2,0,1:T(8,128)(2,1)}), bf16[256,16,128]{2,0,1:T(8,128)(2,1)S(1)}, u32[]{:S(2)}, u32[]{:S(2)}) async-start(bf16[256,16,128]{2,0,1:T(8,128)(2,1)} %bitcast.127), calls=%async_computation | async-start | bytes 2097152 | tf_op jit(solution)/shard_map/all_to_all | solution.py:99
  115.1 4.4 copy-start.3
  130.1 3.2 copy-start.2
  130.1 3.2 copy-start.5
  148.3 3.2 copy-start.2
  148.3 3.2 copy-start.5
  166.5 3.2 copy-start.2
  166.6 3.2 copy-start.5
  184.7 3.2 copy-start.2
  184.7 3.2 copy-start.5
  197.3 7.4 %copy-start.6 = (s32[1,256,2]{1,2,0:T(2,128)S(1)}, s32[1,256,2]{1,2,0:T(2,128)}, u32[]{:S(2)}) copy-start(s32[1,256,2]{1,2,0:T(2,128)} %param.30) | copy-start | bytes 6148
  201.0 34.4 %all-to-all-start.2 = ((bf16[2048,2,128]{2,1,0:T(2,128)(2,1)}), bf16[2048,2,128]{2,1,0:T(2,128)(2,1)S(1)}, u32[]{:S(2)}, u32[]{:S(2)}) async-start(bf16[2048,2,128]{2,1,0:T(2,128)(2,1)} %copy.95), calls=%async_computation.2 | async-start | bytes 2097152 | tf_op jit(solution)/shard_map/all_to_all | solution.py:144
  236.1 6.1 %copy-start.7 = (f32[2048]{0:T(1024)S(1)}, f32[2048]{0:T(1024)}, u32[]{:S(2)}) copy-start(f32[2048]{0:T(1024)} %param.26) | copy-start | bytes 24580
  251.1 95.5 %copy-start.9 = (bf16[1,2048,1024]{2,1,0:T(8,128)(2,1)S(1)}, bf16[1,2048,1024]{2,1,0:T(8,128)(2,1)}, u32[]{:S(2)}) copy-start(bf16[1,2048,1024]{2,1,0:T(8,128)(2,1)} %param.28) | copy-start | bytes 12582916
  346.6 4.5 copy-start.10
  351.1 5.4 %copy-start.11 = (bf16[1,1024,2048]{2,1,0:T(8,128)(2,1)S(1)}, bf16[1,1024,2048]{2,1,0:T(8,128)(2,1)}, u32[]{:S(2)}) copy-start(bf16[1,1024,2048]{2,1,0:T(8,128)(2,1)} %param.29) | copy-start | bytes 12582916
  362.6 5.6 %copy-start.8 = (f32[1,256,2]{1,2,0:T(2,128)S(1)}, f32[1,256,2]{1,2,0:T(2,128)}, u32[]{:S(2)}) copy-start(f32[1,256,2]{1,2,0:T(2,128)} %param.31) | copy-start | bytes 6148
  362.6 96.9 %all-to-all-start.4 = ((bf16[8,128,2048]{2,1,0:T(8,128)(2,1)}), bf16[8,128,2048]{2,1,0:T(8,128)(2,1)}, u32[]{:S(2)}, u32[]{:S(2)}) async-start(bf16[8,128,2048]{2,1,0:T(8,128)(2,1)} %bitcast.152), calls=%async_computation.4 | async-start | bytes 8388608 | tf_op jit(solution)/shard_map/all_to_all | solution.py:167
  467.4 15.6 %copy-start.1 = (bf16[256,256]{1,0:T(8,128)(2,1)S(1)}, bf16[256,256]{1,0:T(8,128)(2,1)}, u32[]{:S(2)}) copy-start(bf16[256,256]{1,0:T(8,128)(2,1)} %param.23) | copy-start | bytes 393220
Sparse Core Ops, SparseCore 0:
  8.9 19.4 all-gather.5
  30.5 57.7 all-gather.3
  90.4 131.3 all-gather.7
where the time goes:
time: 490 us
  waiting for transfers between devices  154 us (31%)
  blocking collectives  151 us (31%)
  matrix products  80.1 us (16%)
  local copies, waits for them, and re-layouts  40 us (8%)
  other arithmetic  30.5 us (6%)
  starting transfers between devices  17.9 us (4%)
  between operations  13.5 us (3%)
    all_to_all x1, blocking collectives, shards(): lax.all_to_all(outgoing, 'sp', split_axis=0, concat_axis=0, tiled=True)  95.5 us
    all_to_all x1, waiting for transfers between devices, shards(): lax.all_to_all(result.reshape(senders, slots_now, width), 'sp', split_axi...  91 us
    all_gather x1, blocking collectives, shards(): lax.all_gather(key_turned, 'sp', axis=0, tiled=True)  55.9 us
    dot_general x4, matrix products, one_block(): jnp.einsum('hbs,shd->bhd', attend, value_heads, preferred_element_type=jn...  36.8 us
    all_to_all x1, waiting for transfers between devices, shards(): lax.all_to_all(attended, 'sp', split_axis=0, concat_axis=1, tiled=True)  28 us
    all_to_all x1, waiting for transfers between devices, shards(): lax.all_to_all(query_turned, 'sp', split_axis=1, concat_axis=0, tiled=True)  17.7 us
    all_gather x1, waiting for transfers between devices, shards(): head_rows = lax.all_gather(out_proj, 'dp', axis=1, tiled=True)  16.1 us
    gather x2, local copies, waits for them, and re-layouts, combine_slots(): jnp.take(flat_back, slot_ids, axis=0).astype(jnp.float32)  12.4 us
  transfers between devices with their start and end apart: 7, of which 4 were waited for; matrix products, arithmetic and copies ran while one was open for 18% of the time, Pallas kernels for 0%

commit v1 on v0

v1 whole, which is shorter than its diff:
```python
import jax
import jax.numpy as jnp
from jax import lax
from jax.experimental import pallas as pl
from jax.experimental.pallas import tpu as pltpu
from jax.sharding import PartitionSpec as P

epsilon = 1e-06
rope_base = 10000.0
masked_score = -1e30


def rotate(values, positions):
    half_width = values.shape[-1] // 2
    frequency = rope_base ** (-jnp.arange(half_width, dtype=jnp.float32) / half_width)
    angles = positions.astype(jnp.float32)[:, None] * frequency[None, :]
    cosine = jnp.cos(angles)
    sine_part = jnp.sin(angles)
    if values.ndim == 3:
        cosine = cosine[:, None, :]
        sine_part = sine_part[:, None, :]
    floats = values.astype(jnp.float32)
    first_half = floats[..., :half_width]
    second_half = floats[..., half_width:]
    turned = jnp.concatenate(
        [
            first_half * cosine - second_half * sine_part,
            second_half * cosine + first_half * sine_part,
        ],
        axis=-1,
    )
    return turned.astype(jnp.bfloat16)


def rms_scaled(values, gain):
    floats = values.astype(jnp.float32)
    return floats * lax.rsqrt(jnp.mean(floats * floats, axis=-1, keepdims=True) + epsilon) * gain


def assign_slots(route_block, experts_all, capacity):
    flat_routes = route_block.reshape(-1)
    onehot = (flat_routes[:, None] == jnp.arange(experts_all, dtype=jnp.int32)[None, :]).astype(
        jnp.int32
    )
    earlier = jnp.cumsum(onehot, axis=0) - onehot
    placed = jnp.sum(earlier * onehot, axis=1)
    return flat_routes * capacity + placed


def one_hot_slots(slot_ids, slots):
    ids = jnp.arange(slots, dtype=jnp.int32)
    return (slot_ids[:, None] == ids[None, :]).astype(jnp.bfloat16)


def attention_kernel(
    heads, nope, block, scale, query_ref, latent_ref, tail_ref, key_up_ref, value_up_ref, out_ref
):
    length = query_ref.shape[0]
    value_width = value_up_ref.shape[1] // heads
    factor = scale * 1.4426950408889634
    keys = jnp.dot(
        latent_ref[...], key_up_ref[...], preferred_element_type=jnp.float32
    ).astype(jnp.bfloat16)
    values = jnp.dot(
        latent_ref[...], value_up_ref[...], preferred_element_type=jnp.float32
    ).astype(jnp.bfloat16)
    rows = lax.broadcasted_iota(jnp.int32, (block, block), 0)
    columns = lax.broadcasted_iota(jnp.int32, (block, block), 1)
    allowed = columns <= rows
    contract_last = (((1,), (1,)), ((), ()))
    for step in range(length // block):
        low = step * block
        high = low + block
        turned = query_ref[low:high, heads * nope :]
        for head in range(heads):
            full_keys = jnp.concatenate(
                [keys[:high, head * nope : (head + 1) * nope], tail_ref[head, :high, :]], axis=1
            )
            full_query = jnp.concatenate(
                [query_ref[low:high, head * nope : (head + 1) * nope], turned], axis=1
            )
            scores = lax.dot_general(
                full_query, full_keys, contract_last, preferred_element_type=jnp.float32
            )
            own = jnp.where(allowed, scores[:, low:], masked_score)
            if step:
                scores = jnp.concatenate([scores[:, :low], own], axis=1)
            else:
                scores = own
            largest = jnp.max(scores, axis=-1, keepdims=True)
            powers = jnp.exp2((scores - largest) * factor)
            total = jnp.sum(powers, axis=-1, keepdims=True)
            picked = jnp.dot(
                powers.astype(jnp.bfloat16),
                values[:high, head * value_width : (head + 1) * value_width],
                preferred_element_type=jnp.float32,
            )
            out_ref[low:high, head * value_width : (head + 1) * value_width] = (
                picked / total
            ).astype(jnp.bfloat16)


def attention(queries, latents, tails, key_up, value_up, nope, block, scale):
    heads = tails.shape[0]
    return pl.pallas_call(
        lambda *refs: attention_kernel(heads, nope, block, scale, *refs),
        out_shape=jax.ShapeDtypeStruct((queries.shape[0], value_up.shape[1]), jnp.bfloat16),
        in_specs=[pl.BlockSpec(memory_space=pltpu.VMEM)] * 5,
        out_specs=pl.BlockSpec(memory_space=pltpu.VMEM),
        compiler_params=pltpu.CompilerParams(vmem_limit_bytes=56 * 1024 * 1024),
    )(queries, latents, tails, key_up, value_up)


def shards(
    query_nope,
    query_rope,
    latent,
    key_rope,
    resid,
    latent_gain,
    key_up,
    value_up,
    out_proj,
    norm_gain,
    expert_gate,
    expert_up,
    expert_down,
    routes,
    route_weight,
):
    tokens_here = latent.shape[1]
    sp_count = lax.axis_size("sp")
    length = tokens_here * sp_count
    heads_all, nope = query_nope.shape[2:]
    turn = query_rope.shape[3]
    heads_here = heads_all // sp_count
    latent_width = latent.shape[2]
    local_pos = lax.axis_index("sp") * tokens_here + jnp.arange(tokens_here, dtype=jnp.int32)
    latent_normed = rms_scaled(latent[0], latent_gain).astype(jnp.bfloat16)
    key_turned = rotate(key_rope[0], local_pos)
    query_turned = rotate(query_rope[0], local_pos)
    all_proj = lax.all_gather(out_proj, ("sp", "dp"))
    cut = latent_width - turn
    first_part = lax.all_gather(latent_normed[:, :cut], "sp", axis=0, tiled=True)
    second_part = lax.all_gather(
        jnp.concatenate([latent_normed[:, cut:], key_turned], axis=1), "sp", axis=0, tiled=True
    )
    all_latent = jnp.concatenate([first_part, second_part[:, :turn]], axis=1)
    all_keyturn = second_part[:, turn:]
    packed_query = jnp.concatenate(
        [
            query_nope[0].reshape(tokens_here, sp_count, heads_here * nope),
            query_turned.reshape(tokens_here, sp_count, heads_here * turn),
        ],
        axis=2,
    ).transpose(1, 0, 2)
    queries = lax.all_to_all(packed_query, "sp", split_axis=0, concat_axis=0, tiled=True)
    queries = queries.reshape(length, -1)
    tails = jnp.stack(
        [
            jnp.pad(all_keyturn, ((0, 0), (head * turn, (heads_here - 1 - head) * turn)))
            for head in range(heads_here)
        ]
    )
    attended = attention(
        queries, all_latent, tails, key_up, value_up, nope, min(256, length), (nope + turn) ** (-0.5)
    )
    token_heads = lax.all_to_all(
        attended.reshape(sp_count, tokens_here, -1), "sp", split_axis=0, concat_axis=0, tiled=True
    )
    dp_count = lax.axis_size("dp")
    all_proj = all_proj.reshape(sp_count, dp_count, out_proj.shape[0], out_proj.shape[1])
    projected = jnp.einsum(
        "stk,sdkn->tdn", token_heads, all_proj, preferred_element_type=jnp.float32
    ).astype(jnp.bfloat16).reshape(tokens_here, -1)
    after_attention = resid[0].astype(jnp.float32) + projected.astype(jnp.float32)
    normed = rms_scaled(after_attention, norm_gain).astype(jnp.bfloat16)
    experts_all = sp_count * expert_gate.shape[0]
    capacity = 4 * tokens_here // experts_all
    slot_ids = assign_slots(routes[0], experts_all, capacity).reshape(tokens_here, 2)
    slots = experts_all * capacity
    first_slots = one_hot_slots(slot_ids[:, 0], slots)
    second_slots = one_hot_slots(slot_ids[:, 1], slots)
    outgoing = lax.dot_general(
        first_slots + second_slots,
        normed,
        (((0,), (0,)), ((), ())),
        preferred_element_type=jnp.float32,
    ).astype(jnp.bfloat16)
    arrived = lax.all_to_all(
        outgoing.reshape(experts_all, capacity, -1), "sp", split_axis=0, concat_axis=0, tiled=True
    )
    senders, slots_now, width = arrived.shape
    rows = arrived.reshape(senders * slots_now, width)
    gate = jnp.dot(rows, expert_gate[0], preferred_element_type=jnp.float32)
    upward = jnp.dot(rows, expert_up[0], preferred_element_type=jnp.float32)
    hidden = (jax.nn.silu(gate) * upward).astype(jnp.bfloat16)
    result = jnp.dot(hidden, expert_down[0], preferred_element_type=jnp.float32).astype(
        jnp.bfloat16
    )
    returned = lax.all_to_all(
        result.reshape(senders, slots_now, width), "sp", split_axis=0, concat_axis=0, tiled=True
    ).reshape(slots, width)
    weights = route_weight[0]
    routed = weights[:, :1] * jnp.dot(
        first_slots, returned, preferred_element_type=jnp.float32
    ) + weights[:, 1:] * jnp.dot(second_slots, returned, preferred_element_type=jnp.float32)
    return (after_attention + routed).astype(jnp.bfloat16)[None]


def solution(mesh):
    return jax.shard_map(
        shards,
        mesh=mesh,
        in_specs=(
            P("dp", "sp", None, None),
            P("dp", "sp", None, None),
            P("dp", "sp", None),
            P("dp", "sp", None),
            P("dp", "sp", None),
            P(),
            P(None, "sp"),
            P(None, "sp"),
            P("sp", "dp"),
            P(),
            P("sp", None, None),
            P("sp", None, None),
            P("sp", None, None),
            P("dp", "sp", None),
            P("dp", "sp", None),
        ),
        out_specs=P("dp", "sp", None),
        check_vma=False,
    )
```

time: 490 us -> 396 us (0.81)
  waiting for transfers between devices: 154 us -> 105 us
  matrix products: 80.1 us -> 31.8 us
  blocking collectives: 151 us -> 199 us
  local copies, waits for them, and re-layouts: 40 us -> 9.49 us
  other arithmetic: 30.5 us -> 7.73 us
  Pallas kernels: 0 us -> 12.1 us
    all_gather x1 -> x2, blocking collectives: 55.9 us -> 111 us  [the longest x1 75.6 us: shards(): lax.all_gather(jnp.concatenate([latent_normed[:, cut:], key_turned], axis...]
    dot_general x15 -> x4, matrix products: 64.1 us -> 15.8 us  [the longest x1 6.04 us: shards(): jnp.einsum('stk,sdkn->tdn', token_heads, all_proj, preferred_element_type...]
    all_to_all x3 -> x2, waiting for transfers between devices: 45.8 us -> 14.2 us  [the longest x1 14.2 us: shards(): lax.all_to_all(attended.reshape(sp_count, tokens_here, -1), 'sp', split_a...]
    gather x3 -> x0, local copies, waits for them, and re-layouts: 18.5 us -> none  [the longest x2 12.4 us: combine_slots(): jnp.take(flat_back, slot_ids, axis=0).astype(jnp.float32)]
    all_gather x3 -> x1, waiting for transfers between devices: 16.1 us -> 0.01 us  [shards(): all_proj = lax.all_gather(out_proj, ('sp', 'dp'))]
    pallas_call x0 -> x1, Pallas kernels: none -> 12.1 us  [attention(): pl.pallas_call(lambda *refs: attention_kernel(heads, nope, block, scale,...]
    reduce_sum x2 -> x0, other arithmetic: 10.2 us -> none  [the longest x1 9.9 us: combine_slots(): return jnp.sum(weights[:, :, None] * picked, axis=1)]
    all_to_all x1, blocking collectives: 95.5 us -> 88.6 us  [shards(): lax.all_to_all(outgoing.reshape(experts_all, capacity, -1), 'sp', split_a...]
  transfers between devices with their start and end apart: 7 -> 4, of which waited for: 4 -> 2; matrix products, arithmetic and copies ran while one was open for 18% -> 3% of each run, Pallas kernels for 0% -> 3%
where the time goes in v1:
time: 396 us
  blocking collectives  199 us (50%)
  waiting for transfers between devices  105 us (27%)
  matrix products  31.8 us (8%)
  starting transfers between devices  16.4 us (4%)
  between operations  13.7 us (3%)
  Pallas kernels  12.1 us (3%)
  local copies, waits for them, and re-layouts  9.49 us (2%)
  other arithmetic  7.73 us (2%)
    all_to_all x1, waiting for transfers between devices, shards(): lax.all_to_all(result.reshape(senders, slots_now, width), 'sp', split_axi...  90 us
    all_to_all x1, blocking collectives, shards(): lax.all_to_all(outgoing.reshape(experts_all, capacity, -1), 'sp', split_a...  88.6 us
    all_gather x1, blocking collectives, shards(): lax.all_gather(jnp.concatenate([latent_normed[:, cut:], key_turned], axis...  75.6 us
    all_gather x1, blocking collectives, shards(): lax.all_gather(latent_normed[:, :cut], 'sp', axis=0, tiled=True)  35.1 us
    all_to_all x1, waiting for transfers between devices, shards(): lax.all_to_all(attended.reshape(sp_count, tokens_here, -1), 'sp', split_a...  14.2 us
    pallas_call x1, Pallas kernels, attention(): pl.pallas_call(lambda *refs: attention_kernel(heads, nope, block, scale,...  12.1 us
  transfers between devices with their start and end apart: 4, of which 2 were waited for; matrix products, arithmetic and copies ran while one was open for 3% of the time, Pallas kernels for 3%

profile of v1, /device:TPU:0, one launch (start us, length us, event | category | flops | bytes accessed | tf_op | source)
XLA Modules:
  0.0 395.5 jit_solution(15399069869424188910)
XLA Ops:
  6.5 0.7 all-gather.3.cloned.1.call-update
  7.3 0.9 copy.48
  8.2 0.6 subtract_convert_fusion.1
  8.8 0.1 copy.44
  8.8 0.1 copy.45
  8.9 1.2 bitcast_convert_fusion.1
  10.1 0.2 subtract_convert_fusion
  10.3 0.3 copy.47
  10.6 0.4 reshape_squeeze.4
  11.0 0.2 copy.46
  11.2 1.4 maximum_bitcast_fusion
  12.6 7.3 %all-to-all-start = ((bf16[8,256,384]{2,1,0:T(8,128)(2,1)}), bf16[8,256,384]{2,1,0:T(8,128)(2,1)S(1)}, u32[]{:S(2)}, u32[]{:S(2)}) async-start(bf16[8,256,384]{2,1,0:T(8,128)(2,1)} %maximum_bitcast_fusion), calls=%async_computation | async-start | bytes 3145728 | tf_op jit(solution)/shard_map/all_to_all | solution.py:157
  19.9 0.1 fusion.28
  20.1 0.1 fusion.30
  20.2 0.1 slice.59
  20.3 0.1 pad_maximum_fusion.3
  20.4 75.6 %all_gather.13 = bf16[2048,128]{1,0:T(8,128)(2,1)S(1)} all-gather(bf16[256,128]{1,0:T(8,128)(2,1)S(1)} %pad_maximum_fusion.3), channel_id=1, replica_groups=mesh['sp'=8,'dp'=4] {'sp'}, dimensions={0}, use_global_device_ids=true | all-gather | bytes 589824 | tf_op jit(solution)/shard_map/all_gather | solution.py:145
  96.0 0.2 fusion.34
  96.2 0.3 pad_bitcast_fusion.1
  96.5 1.1 pad_maximum_fusion.1.refs_2_
  97.6 35.1 %all_gather.12 = bf16[2048,192]{1,0:T(8,128)(2,1)S(1)} all-gather(bf16[256,192]{1,0:T(8,128)(2,1)S(1)} %bitcast.92), channel_id=1, replica_groups=mesh['sp'=8,'dp'=4] {'sp'}, dimensions={0}, use_global_device_ids=true | all-gather | bytes 884736 | tf_op jit(solution)/shard_map/all_gather | solution.py:144
  132.7 1.3 pad_maximum_fusion.refs_1_
  134.0 1.2 copy-done.1
  135.2 12.1 %shard_map.145 = bf16[2048,256]{1,0:T(8,128)(2,1)} custom-call(bf16[2048,384]{1,0:T(8,128)(2,1)} %bitcast.86, bf16[2048,256]{1,0:T(8,128)(2,1)} %pad_maximum_fusion.refs_1_, bf16[2,2048,128]{2,1,0:T(8,128)(2,1)} %pad_maximum_fusion.1.refs_2_, bf16[256,256]{1,0:T(8,128)(2,1)} %refs_3_.1, bf16[256,256]{1,0:T(8,128)(2,1)} %refs_4_.1), custom_call_target="tpu_custom_call" | custom-call | tf_op jit(solution)/shard_map/pallas_call | solution.py:105
  147.4 4.2 %all-to-all-start.1 = ((bf16[8,256,256]{2,1,0:T(8,128)(2,1)}), bf16[8,256,256]{2,1,0:T(8,128)(2,1)S(1)}, u32[]{:S(2)}, u32[]{:S(2)}) async-start(bf16[8,256,256]{2,1,0:T(8,128)(2,1)} %bitcast.87), calls=%async_computation.1 | async-start | bytes 2097152 | tf_op jit(solution)/shard_map/all_to_all | solution.py:168
  151.6 0.1 copy.52
  151.7 0.1 eq.59
  151.8 0.1 eq.55
  152.0 1.1 reduce-window.6
  153.1 0.2 slice_reduce_fusion.2
  153.4 0.1 fusion.32
  153.5 0.1 reduce_sum.31
  153.7 0.2 slice_reduce_fusion.1
  153.9 14.2 %all-to-all-done.1 = bf16[8,256,256]{2,1,0:T(8,128)(2,1)S(1)} async-done(((bf16[8,256,256]{2,1,0:T(8,128)(2,1)}), bf16[8,256,256]{2,1,0:T(8,128)(2,1)S(1)}, u32[]{:S(2)}, u32[]{:S(2)}) %all-to-all-start.1) | async-done | bytes 1048608 | tf_op jit(solution)/shard_map/all_to_all | solution.py:168
  168.1 1.0 copy-done.3
  169.0 6.0 %fusion.15 = f32[256,4,512]{2,0,1:T(8,128)S(1)} fusion(bf16[8,4,256,512]{3,2,1,0:T(8,128)(2,1)} %bitcast.96, bf16[8,256,256]{2,1,0:T(8,128)(2,1)} %copy-done.3), kind=kOutput, calls=%fused_computation.20 | convolution fusion | flops 2148532224 | bytes 11534336 | tf_op jit(solution)/shard_map/stk,sdkn->tdn/dot_general | solution.py:173
  175.1 1.9 copy.50
  177.0 1.9 copy.51
  178.9 0.4 multiply_reduce_fusion
  179.3 1.6 convolution_convert_fusion
  180.9 88.6 %all_to_all.20 = bf16[8,128,2048]{2,1,0:T(8,128)(2,1)S(1)} all-to-all(bf16[8,128,2048]{2,1,0:T(8,128)(2,1)S(1)} %bitcast.84), channel_id=1, replica_groups=mesh['sp'=8,'dp'=4] {'sp'}, dimensions={0} | all-to-all | bytes 8388608 | tf_op jit(solution)/shard_map/all_to_all | solution.py:190
  269.5 4.5 %fusion.2 = f32[1024,1024]{1,0:T(8,128)S(1)} fusion(bf16[1024,2048]{1,0:T(8,128)(2,1)S(1)} %bitcast.89, bf16[1,2048,1024]{2,1,0:T(8,128)(2,1)S(1)} %copy-done.9), kind=kOutput, calls=%fused_computation.2 | convolution fusion | flops 4294967296 | bytes 12582912 | tf_op jit(solution)/shard_map/dot_general | solution.py:196
  274.0 5.4 %multiply_convert_fusion = bf16[1024,1024]{1,0:T(8,128)(2,1)S(1)} fusion(f32[1024,1024]{1,0:T(8,128)S(1)} %fusion.2, bf16[1024,2048]{1,0:T(8,128)(2,1)S(1)} %bitcast.90, bf16[1,2048,1024]{2,1,0:T(8,128)(2,1)S(1)} %copy-done.10), kind=kOutput, calls=%fused_computation.6 | convolution fusion | flops 4301258752 | bytes 14680064 | tf_op jit(solution)/shard_map/dot_general | solution.py:195
  279.4 6.1 %fusion.6 = bf16[1024,2048]{1,0:T(8,128)(2,1)} fusion(bf16[1024,1024]{1,0:T(8,128)(2,1)S(1)} %multiply_convert_fusion, bf16[1,1024,2048]{2,1,0:T(8,128)(2,1)S(1)} %copy-done.11), kind=kOutput, calls=%fused_computation.8 | convolution fusion | flops 4297064448 | bytes 10485760 | tf_op jit(solution)/shard_map/dot_general | solution.py:198
  285.5 4.9 %all-to-all-start.3 = ((bf16[8,128,2048]{2,1,0:T(8,128)(2,1)}), bf16[8,128,2048]{2,1,0:T(8,128)(2,1)}, u32[]{:S(2)}, u32[]{:S(2)}) async-start(bf16[8,128,2048]{2,1,0:T(8,128)(2,1)} %bitcast.88), calls=%async_computation.3 | async-start | bytes 8388608 | tf_op jit(solution)/shard_map/all_to_all | solution.py:201
  290.5 90.0 %all-to-all-done.3 = bf16[8,128,2048]{2,1,0:T(8,128)(2,1)} async-done(((bf16[8,128,2048]{2,1,0:T(8,128)(2,1)}), bf16[8,128,2048]{2,1,0:T(8,128)(2,1)}, u32[]{:S(2)}, u32[]{:S(2)}) %all-to-all-start.3) | async-done | bytes 4194336 | tf_op jit(solution)/shard_map/all_to_all | solution.py:201
  380.5 3.5 convolution_multiply_fusion
  384.0 4.7 %fusion.14 = bf16[1,256,2048]{2,1,0:T(8,128)(2,1)} fusion(f32[256,2048]{1,0:T(8,128)S(1)} %convolution_multiply_fusion, bf16[1024,2048]{1,0:T(8,128)(2,1)} %bitcast.29, f32[256]{0:T(256)S(1)} %bitcast.93, f32[256,2048]{1,0:T(8,128)S(1)} %copy.51, bf16[1,256,2048]{2,1,0:T(8,128)(2,1)S(1)} %copy-done, s32[256]{0:T(256)S(1)} %get-tuple-element.5), kind=kOutput, calls=%fused_computation.14 | convolution fusion | flops 1077149696 | bytes 10487808 | tf_op jit(solution)/shard_map/dot_general | solution.py:205
  (36 shorter events, 0.2 us)
Async XLA Ops:
  6.5 4.0 %copy-start.2 = (bf16[1,256,16,128]{3,2,1,0:T(8,128)(2,1)S(1)}, bf16[1,256,16,128]{3,2,1,0:T(8,128)(2,1)}, u32[]{:S(2)}) copy-start(bf16[1,256,16,128]{3,2,1,0:T(8,128)(2,1)} %param.15) | copy-start | bytes 3145732
  6.5 161.5 %all-gather.3.cloned.1.call-start = ((), (), s32[]{:S(2)}) async-start(), calls=%async_computation.4 | async-start | bytes 8650752 | tf_op jit(solution)/shard_map/all_gather | solution.py:142
  11.0 9.0 %copy-start.4 = (bf16[1,256,256]{2,1,0:T(8,128)(2,1)S(1)}, bf16[1,256,256]{2,1,0:T(8,128)(2,1)}, u32[]{:S(2)}) copy-start(bf16[1,256,256]{2,1,0:T(8,128)(2,1)} %param.17) | copy-start | bytes 393220
  11.0 9.1 %copy-start.8 = (f32[256]{0:T(256)S(1)}, f32[256]{0:T(256)}, u32[]{:S(2)}) copy-start(f32[256]{0:T(256)} %param.20) | copy-start | bytes 3076
  12.6 121.4 %all-to-all-start = ((bf16[8,256,384]{2,1,0:T(8,128)(2,1)}), bf16[8,256,384]{2,1,0:T(8,128)(2,1)S(1)}, u32[]{:S(2)}, u32[]{:S(2)}) async-start(bf16[8,256,384]{2,1,0:T(8,128)(2,1)} %maximum_bitcast_fusion), calls=%async_computation | async-start | bytes 3145728 | tf_op jit(solution)/shard_map/all_to_all | solution.py:157
  134.0 17.5 %copy-start.6 = (s32[1,256,2]{1,2,0:T(2,128)S(1)}, s32[1,256,2]{1,2,0:T(2,128)}, u32[]{:S(2)}) copy-start(s32[1,256,2]{1,2,0:T(2,128)} %param.28) | copy-start | bytes 6148
  134.0 1.2 copy-start.1
  147.4 20.7 %all-to-all-start.1 = ((bf16[8,256,256]{2,1,0:T(8,128)(2,1)}), bf16[8,256,256]{2,1,0:T(8,128)(2,1)S(1)}, u32[]{:S(2)}, u32[]{:S(2)}) async-start(bf16[8,256,256]{2,1,0:T(8,128)(2,1)} %bitcast.87), calls=%async_computation.1 | async-start | bytes 2097152 | tf_op jit(solution)/shard_map/all_to_all | solution.py:168
  168.1 1.0 copy-start.3
  175.1 3.8 copy-start
  177.0 2.3 copy-start.5
  180.9 88.6 %copy-start.9 = (bf16[1,2048,1024]{2,1,0:T(8,128)(2,1)S(1)}, bf16[1,2048,1024]{2,1,0:T(8,128)(2,1)}, u32[]{:S(2)}) copy-start(bf16[1,2048,1024]{2,1,0:T(8,128)(2,1)} %param.26) | copy-start | bytes 12582916
  269.5 4.5 %copy-start.10 = (bf16[1,2048,1024]{2,1,0:T(8,128)(2,1)S(1)}, bf16[1,2048,1024]{2,1,0:T(8,128)(2,1)}, u32[]{:S(2)}) copy-start(bf16[1,2048,1024]{2,1,0:T(8,128)(2,1)} %param.25) | copy-start | bytes 12582916
  274.0 5.4 %copy-start.11 = (bf16[1,1024,2048]{2,1,0:T(8,128)(2,1)S(1)}, bf16[1,1024,2048]{2,1,0:T(8,128)(2,1)}, u32[]{:S(2)}) copy-start(bf16[1,1024,2048]{2,1,0:T(8,128)(2,1)} %param.27) | copy-start | bytes 12582916
  285.5 4.9 %copy-start.7 = (f32[1,256,2]{1,2,0:T(2,128)S(1)}, f32[1,256,2]{1,2,0:T(2,128)}, u32[]{:S(2)}) copy-start(f32[1,256,2]{1,2,0:T(2,128)} %param.29) | copy-start | bytes 6148
  285.5 95.0 %all-to-all-start.3 = ((bf16[8,128,2048]{2,1,0:T(8,128)(2,1)}), bf16[8,128,2048]{2,1,0:T(8,128)(2,1)}, u32[]{:S(2)}, u32[]{:S(2)}) async-start(bf16[8,128,2048]{2,1,0:T(8,128)(2,1)} %bitcast.88), calls=%async_computation.3 | async-start | bytes 8388608 | tf_op jit(solution)/shard_map/all_to_all | solution.py:201
Sparse Core Ops, SparseCore 0:
  10.2 115.0 all-gather.2

commit v2 on v1

--- a/solution.py
+++ b/solution.py
@@ -52,18 +52,95 @@
     return (slot_ids[:, None] == ids[None, :]).astype(jnp.bfloat16)
 
 
-def attention_kernel(
-    heads, nope, block, scale, query_ref, latent_ref, tail_ref, key_up_ref, value_up_ref, out_ref
-):
+def ring_gather(local):
+    count = lax.axis_size("sp")
+    order = list(range(0, count, 2)) + list(range(count - 1, 0, -2))
+    onward = [(order[i], order[(i + 1) % count]) for i in range(count)]
+    backward = [(target, source) for source, target in onward]
+    place = jnp.array([order.index(i) for i in range(count)])[lax.axis_index("sp")]
+    blocks = [local]
+    offsets = [0]
+    ahead = behind = local
+    for step in range(1, count // 2 + 1):
+        ahead = lax.ppermute(ahead, "sp", onward)
+        blocks.append(ahead)
+        offsets.append(-step)
+        if step <= (count - 1) // 2:
+            behind = lax.ppermute(behind, "sp", backward)
+            blocks.append(behind)
+            offsets.append(step)
+    sources = jnp.array(order)[(place + jnp.array(offsets)) % count]
+    return blocks, sources.astype(jnp.int32)
+
+
+def column_gather(local):
+    count = lax.axis_size("dp")
+    here = lax.axis_index("dp")
+    across = [(i, (i + 2) % count) for i in range(count)]
+    swap = [(i, i ^ 1) for i in range(count)]
+    pieces = [local]
+    sources = [here]
+    current = local
+    for step in range(1, count // 2):
+        current = lax.ppermute(current, "dp", across)
+        pieces.append(current)
+        sources.append((here - 2 * step) % count)
+    for step in range(count // 2):
+        pieces.append(lax.ppermute(pieces[step], "dp", swap))
+        sources.append(((here ^ 1) - 2 * step) % count)
+    return pieces, jnp.stack(sources).astype(jnp.int32)
+
+
+def projection_kernel(count, sources_ref, columns_ref, heads_ref, *refs):
+    pieces, out_ref = refs[:-1], refs[-1]
+    width = pieces[0].shape[2]
+    heads = [heads_ref[sources_ref[step]] for step in range(count)]
+    for index, piece in enumerate(pieces):
+        total = jnp.dot(heads[0], piece[0], preferred_element_type=jnp.float32)
+        for step in range(1, count):
+            total += jnp.dot(heads[step], piece[step], preferred_element_type=jnp.float32)
+        start = pl.multiple_of(columns_ref[index] * width, width)
+        out_ref[:, pl.ds(start, width)] = total.astype(jnp.bfloat16)
+
+
+def project(sources, columns, token_heads, pieces):
+    count, rows, _ = token_heads.shape
+    width = len(pieces) * pieces[0].shape[2]
+    return pl.pallas_call(
+        lambda *refs: projection_kernel(count, *refs),
+        out_shape=jax.ShapeDtypeStruct((rows, width), jnp.bfloat16),
+        in_specs=[pl.BlockSpec(memory_space=pltpu.SMEM)] * 2
+        + [pl.BlockSpec(memory_space=pltpu.VMEM)] * (1 + len(pieces)),
+        out_specs=pl.BlockSpec(memory_space=pltpu.VMEM),
+        compiler_params=pltpu.CompilerParams(vmem_limit_bytes=48 * 1024 * 1024),
+    )(sources, columns, token_heads, *pieces)
+
+
+def attention_kernel(heads, nope, block, scale, count, *refs):
+    sources_ref, query_ref, key_up_ref, value_up_ref = refs[:4]
+    latent_refs = refs[4 : 4 + count]
+    out_ref, keys, values, tail_ref = refs[4 + count :]
     length = query_ref.shape[0]
     value_width = value_up_ref.shape[1] // heads
     factor = scale * 1.4426950408889634
-    keys = jnp.dot(
-        latent_ref[...], key_up_ref[...], preferred_element_type=jnp.float32
-    ).astype(jnp.bfloat16)
-    values = jnp.dot(
-        latent_ref[...], value_up_ref[...], preferred_element_type=jnp.float32
-    ).astype(jnp.bfloat16)
+    latent_width = key_up_ref.shape[0]
+    for step in range(count):
+        tokens, packed_width = latent_refs[step].shape
+        turn = packed_width - latent_width
+        start = pl.multiple_of(sources_ref[step] * tokens, tokens)
+        latent = latent_refs[step][:, :latent_width]
+        key_turn = latent_refs[step][:, latent_width:]
+        keys[pl.ds(start, tokens), :] = jnp.dot(
+            latent, key_up_ref[...], preferred_element_type=jnp.float32
+        ).astype(jnp.bfloat16)
+        values[pl.ds(start, tokens), :] = jnp.dot(
+            latent, value_up_ref[...], preferred_element_type=jnp.float32
+        ).astype(jnp.bfloat16)
+        blank = jnp.zeros((tokens, turn), jnp.bfloat16)
+        for head in range(heads):
+            tail_ref[head, pl.ds(start, tokens), :] = jnp.concatenate(
+                [key_turn if other == head else blank for other in range(heads)], axis=1
+            )
     rows = lax.broadcasted_iota(jnp.int32, (block, block), 0)
     columns = lax.broadcasted_iota(jnp.int32, (block, block), 1)
     allowed = columns <= rows
@@ -100,15 +177,22 @@
             ).astype(jnp.bfloat16)
 
 
-def attention(queries, latents, tails, key_up, value_up, nope, block, scale):
-    heads = tails.shape[0]
+def attention(sources, queries, blocks, key_up, value_up, heads, nope, block, scale):
+    length, packed_width = queries.shape
+    count = len(blocks)
     return pl.pallas_call(
-        lambda *refs: attention_kernel(heads, nope, block, scale, *refs),
-        out_shape=jax.ShapeDtypeStruct((queries.shape[0], value_up.shape[1]), jnp.bfloat16),
-        in_specs=[pl.BlockSpec(memory_space=pltpu.VMEM)] * 5,
+        lambda *refs: attention_kernel(heads, nope, block, scale, count, *refs),
+        out_shape=jax.ShapeDtypeStruct((length, value_up.shape[1]), jnp.bfloat16),
+        in_specs=[pl.BlockSpec(memory_space=pltpu.SMEM)]
+        + [pl.BlockSpec(memory_space=pltpu.VMEM)] * (3 + count),
         out_specs=pl.BlockSpec(memory_space=pltpu.VMEM),
+        scratch_shapes=[
+            pltpu.VMEM((length, key_up.shape[1]), jnp.bfloat16),
+            pltpu.VMEM((length, value_up.shape[1]), jnp.bfloat16),
+            pltpu.VMEM((heads, length, packed_width - heads * nope), jnp.bfloat16),
+        ],
         compiler_params=pltpu.CompilerParams(vmem_limit_bytes=56 * 1024 * 1024),
-    )(queries, latents, tails, key_up, value_up)
+    )(sources, queries, key_up, value_up, *blocks)
 
 
 def shards(
@@ -134,19 +218,13 @@
     heads_all, nope = query_nope.shape[2:]
     turn = query_rope.shape[3]
     heads_here = heads_all // sp_count
-    latent_width = latent.shape[2]
     local_pos = lax.axis_index("sp") * tokens_here + jnp.arange(tokens_here, dtype=jnp.int32)
     latent_normed = rms_scaled(latent[0], latent_gain).astype(jnp.bfloat16)
     key_turned = rotate(key_rope[0], local_pos)
     query_turned = rotate(query_rope[0], local_pos)
-    all_proj = lax.all_gather(out_proj, ("sp", "dp"))
-    cut = latent_width - turn
-    first_part = lax.all_gather(latent_normed[:, :cut], "sp", axis=0, tiled=True)
-    second_part = lax.all_gather(
-        jnp.concatenate([latent_normed[:, cut:], key_turned], axis=1), "sp", axis=0, tiled=True
-    )
-    all_latent = jnp.concatenate([first_part, second_part[:, :turn]], axis=1)
-    all_keyturn = second_part[:, turn:]
+    latent_blocks, sources = ring_gather(jnp.concatenate([latent_normed, key_turned], axis=1))
+    row_blocks, _ = ring_gather(out_proj)
+    pieces, columns = column_gather(jnp.stack(row_blocks))
     packed_query = jnp.concatenate(
         [
             query_nope[0].reshape(tokens_here, sp_count, heads_here * nope),
@@ -156,23 +234,21 @@
     ).transpose(1, 0, 2)
     queries = lax.all_to_all(packed_query, "sp", split_axis=0, concat_axis=0, tiled=True)
     queries = queries.reshape(length, -1)
-    tails = jnp.stack(
-        [
-            jnp.pad(all_keyturn, ((0, 0), (head * turn, (heads_here - 1 - head) * turn)))
-            for head in range(heads_here)
-        ]
-    )
     attended = attention(
-        queries, all_latent, tails, key_up, value_up, nope, min(256, length), (nope + turn) ** (-0.5)
+        sources,
+        queries,
+        latent_blocks,
+        key_up,
+        value_up,
+        heads_here,
+        nope,
+        min(256, length),
+        (nope + turn) ** (-0.5),
     )
     token_heads = lax.all_to_all(
         attended.reshape(sp_count, tokens_here, -1), "sp", split_axis=0, concat_axis=0, tiled=True
     )
-    dp_count = lax.axis_size("dp")
-    all_proj = all_proj.reshape(sp_count, dp_count, out_proj.shape[0], out_proj.shape[1])
-    projected = jnp.einsum(
-        "stk,sdkn->tdn", token_heads, all_proj, preferred_element_type=jnp.float32
-    ).astype(jnp.bfloat16).reshape(tokens_here, -1)
+    projected = project(sources, columns, token_heads, pieces)
     after_attention = resid[0].astype(jnp.float32) + projected.astype(jnp.float32)
     normed = rms_scaled(after_attention, norm_gain).astype(jnp.bfloat16)
     experts_all = sp_count * expert_gate.shape[0]

time: 396 us -> 391 us (0.987)
  blocking collectives: 199 us -> 97 us
  waiting for transfers between devices: 105 us -> 191 us
  starting transfers between devices: 16.4 us -> 42.4 us
  between operations: 13.7 us -> 0.54 us
  matrix products: 31.8 us -> 25.7 us
  Pallas kernels: 12.1 us -> 17.7 us
    all_gather x2 -> x0, blocking collectives: 111 us -> none  [the longest x1 75.6 us: shards(): lax.all_gather(jnp.concatenate([latent_normed[:, cut:], key_turned], axis...]
    ppermute x0 -> x17, waiting for transfers between devices: none -> 75.5 us  [the longest x8 52.3 us: ring_gather(): ahead = lax.ppermute(ahead, 'sp', onward)]
    ppermute x0 -> x17, starting transfers between devices: none -> 25.7 us  [the longest x8 21.7 us: ring_gather(): ahead = lax.ppermute(ahead, 'sp', onward)]
    all_to_all x1, waiting for transfers between devices: 14.2 us -> 24 us  [shards(): lax.all_to_all(attended.reshape(sp_count, tokens_here, -1), 'sp', split_a...]
    all_to_all x1, blocking collectives: 88.6 us -> 97 us  [shards(): lax.all_to_all(outgoing.reshape(experts_all, capacity, -1), 'sp', split_a...]
    dot_general x1 -> x0, matrix products: 6.04 us -> none  [shards(): jnp.einsum('stk,sdkn->tdn', token_heads, all_proj, preferred_element_type...]
    pallas_call x0 -> x1, Pallas kernels: none -> 5.27 us  [project(): pl.pallas_call(lambda *refs: projection_kernel(count, *refs), out_shape=j...]
  transfers between devices with their start and end apart: 4 -> 20, of which waited for: 2 -> 11; matrix products, arithmetic and copies ran while one was open for 3% -> 3% of each run, Pallas kernels for 3% -> 3%
where the time goes in v2:
time: 391 us; the launch traced here: 390 us
  waiting for transfers between devices  191 us (49%)
  blocking collectives  97 us (25%)
  starting transfers between devices  42.4 us (11%)
  matrix products  25.7 us (7%)
  Pallas kernels  17.7 us (5%)
  local copies, waits for them, and re-layouts  9.01 us (2%)
  other arithmetic  6.05 us (2%)
    all_to_all x1, blocking collectives, shards(): lax.all_to_all(outgoing.reshape(experts_all, capacity, -1), 'sp', split_a...  97 us
    all_to_all x1, waiting for transfers between devices, shards(): lax.all_to_all(result.reshape(senders, slots_now, width), 'sp', split_axi...  91.9 us
    ppermute x8, waiting for transfers between devices, ring_gather(): ahead = lax.ppermute(ahead, 'sp', onward)  52.3 us
    all_to_all x1, waiting for transfers between devices, shards(): lax.all_to_all(attended.reshape(sp_count, tokens_here, -1), 'sp', split_a...  24 us
    ppermute x1, waiting for transfers between devices, column_gather(): current = lax.ppermute(current, 'dp', across)  22.4 us
    ppermute x8, starting transfers between devices, ring_gather(): ahead = lax.ppermute(ahead, 'sp', onward)  21.7 us
    pallas_call x1, Pallas kernels, attention(): pl.pallas_call(lambda *refs: attention_kernel(heads, nope, block, scale,...  12.4 us
  transfers between devices with their start and end apart: 20, of which 11 were waited for; matrix products, arithmetic and copies ran while one was open for 3% of the time, Pallas kernels for 3%

profile of v2, /device:TPU:0, one launch (start us, length us, event | category | flops | bytes accessed | tf_op | source)
XLA Modules:
  0.0 389.8 jit_solution(10385105752571643581)
XLA Ops:
  0.0 3.1 collective-permute-start.7
  3.1 0.9 copy.45
  4.0 0.6 subtract_convert_fusion.1
  4.7 1.2 bitcast_convert_fusion
  6.4 0.7 copy-done.4
  7.1 0.4 reshape_squeeze.4
  7.7 1.3 maximum_bitcast_fusion
  9.0 6.4 %all-to-all-start = ((bf16[8,256,384]{2,1,0:T(8,128)(2,1)}), bf16[8,256,384]{2,1,0:T(8,128)(2,1)}, u32[]{:S(2)}, u32[]{:S(2)}) async-start(bf16[8,256,384]{2,1,0:T(8,128)(2,1)} %maximum_bitcast_fusion), calls=%async_computation | async-start | bytes 3145728 | tf_op jit(solution)/shard_map/all_to_all | solution.py:235
  15.5 2.1 collective-permute-start.9
  17.5 1.0 bitcast_dynamic-update-slice_fusion.6
  18.7 27.4 %collective-permute-done.9 = bf16[256,512]{1,0:T(8,128)(2,1)S(1)} collective-permute-done((bf16[256,512]{1,0:T(8,128)(2,1)}, bf16[256,512]{1,0:T(8,128)(2,1)S(1)}, u32[]{:S(2)}, u32[]{:S(2)}) %collective-permute-start.9) | collective-permute-done | bytes 262176 | tf_op jit(solution)/shard_map/ppermute | solution.py:65
  46.1 9.9 %collective-permute-start.11 = (bf16[256,512]{1,0:T(8,128)(2,1)S(1)}, bf16[256,512]{1,0:T(8,128)(2,1)S(1)}, u32[]{:S(2)}, u32[]{:S(2)}) collective-permute-start(bf16[256,512]{1,0:T(8,128)(2,1)S(1)} %collective-permute-done.9), channel_id=1, source_target_pairs={{0,8},{8,16},{16,24},{24,28},{28,20},{20,12},{12,4},{4,0},{1,9},{9... | collective-permute-start | bytes 786440 | tf_op jit(solution)/shard_map/ppermute | solution.py:65
  56.2 5.6 %collective-permute-done.11 = bf16[256,512]{1,0:T(8,128)(2,1)S(1)} collective-permute-done((bf16[256,512]{1,0:T(8,128)(2,1)S(1)}, bf16[256,512]{1,0:T(8,128)(2,1)S(1)}, u32[]{:S(2)}, u32[]{:S(2)}) %collective-permute-start.11) | collective-permute-done | bytes 262176 | tf_op jit(solution)/shard_map/ppermute | solution.py:65
  61.8 2.5 collective-permute-start.13
  64.3 0.4 collective-permute-done.12
  64.8 5.3 %collective-permute-done.13 = bf16[256,512]{1,0:T(8,128)(2,1)S(1)} collective-permute-done((bf16[256,512]{1,0:T(8,128)(2,1)S(1)}, bf16[256,512]{1,0:T(8,128)(2,1)S(1)}, u32[]{:S(2)}, u32[]{:S(2)}) %collective-permute-start.13) | collective-permute-done | bytes 262176 | tf_op jit(solution)/shard_map/ppermute | solution.py:65
  70.1 1.6 collective-permute-start.14
  72.0 1.7 collective-permute-start
  73.7 0.4 collective-permute-start.1
  74.1 4.1 %collective-permute-done.refs_5_ = bf16[256,320]{1,0:T(8,128)(2,1)S(1)} collective-permute-done((bf16[256,320]{1,0:T(8,128)(2,1)S(1)}, bf16[256,320]{1,0:T(8,128)(2,1)S(1)}, u32[]{:S(2)}, u32[]{:S(2)}) %collective-permute-start) | collective-permute-done | bytes 163872 | tf_op jit(solution)/shard_map/ppermute | solution.py:65
  78.2 1.3 collective-permute-start.2
  79.5 0.3 collective-permute-done.1.refs_6_
  79.8 0.5 collective-permute-start.3
  80.3 4.8 %collective-permute-done.2.refs_7_ = bf16[256,320]{1,0:T(8,128)(2,1)S(1)} collective-permute-done((bf16[256,320]{1,0:T(8,128)(2,1)S(1)}, bf16[256,320]{1,0:T(8,128)(2,1)S(1)}, u32[]{:S(2)}, u32[]{:S(2)}) %collective-permute-start.2) | collective-permute-done | bytes 163872 | tf_op jit(solution)/shard_map/ppermute | solution.py:65
  85.1 0.9 collective-permute-start.4
  86.0 0.6 dynamic_slice.3
  86.6 1.4 collective-permute-start.5
  88.0 5.0 %collective-permute-done.4.refs_9_ = bf16[256,320]{1,0:T(8,128)(2,1)S(1)} collective-permute-done((bf16[256,320]{1,0:T(8,128)(2,1)S(1)}, bf16[256,320]{1,0:T(8,128)(2,1)S(1)}, u32[]{:S(2)}, u32[]{:S(2)}) %collective-permute-start.4) | collective-permute-done | bytes 163872 | tf_op jit(solution)/shard_map/ppermute | solution.py:65
  93.3 22.4 %collective-permute-done.14.refs_4_ = bf16[8,256,512]{2,1,0:T(8,128)(2,1)} collective-permute-done((bf16[8,256,512]{2,1,0:T(8,128)(2,1)S(1)}, bf16[8,256,512]{2,1,0:T(8,128)(2,1)}, u32[]{:S(2)}, u32[]{:S(2)}) %collective-permute-start.14) | collective-permute-done | bytes 2097184 | tf_op jit(solution)/shard_map/ppermute | solution.py:85
  115.7 0.7 compare_select_fusion
  116.4 1.1 gather_fusion
  117.7 0.6 copy-done.14
  118.3 12.4 %shard_map.172 = bf16[2048,256]{1,0:T(8,128)(2,1)} custom-call(s32[8]{0:T(128)} %gather_fusion, bf16[2048,384]{1,0:T(8,128)(2,1)} %bitcast.10.refs_1_, bf16[256,256]{1,0:T(8,128)(2,1)} %refs_2_.1, bf16[256,256]{1,0:T(8,128)(2,1)} %refs_3_.1, bf16[256,320]{1,0:T(8,128)(2,1)} %copy-done.6, bf16[256,320]{1,0:T(8,128)(2,1)} %copy-done.9, ...), custom_call_target="tpu_custom_call" | custom-call | tf_op jit(solution)/shard_map/pallas_call | solution.py:183
  130.7 5.3 %all-to-all-start.1 = ((bf16[8,256,256]{2,1,0:T(8,128)(2,1)}), bf16[8,256,256]{2,1,0:T(8,128)(2,1)S(1)}, u32[]{:S(2)}, u32[]{:S(2)}) async-start(bf16[8,256,256]{2,1,0:T(8,128)(2,1)} %bitcast.83), calls=%async_computation.1 | async-start | bytes 2097152 | tf_op jit(solution)/shard_map/all_to_all | solution.py:248
  136.5 1.1 reduce-window.6
  138.5 24.0 %all-to-all-done.1.refs_2_ = bf16[8,256,256]{2,1,0:T(8,128)(2,1)S(1)} async-done(((bf16[8,256,256]{2,1,0:T(8,128)(2,1)}), bf16[8,256,256]{2,1,0:T(8,128)(2,1)S(1)}, u32[]{:S(2)}, u32[]{:S(2)}) %all-to-all-start.1) | async-done | bytes 1048608 | tf_op jit(solution)/shard_map/all_to_all | solution.py:248
  162.5 1.6 copy-done.1
  164.1 5.3 %shard_map.173 = bf16[256,2048]{1,0:T(8,128)(2,1)S(1)} custom-call(s32[8]{0:T(128)S(1)} %copy-done.2, s32[4]{0:T(128)S(1)} %pad_add_fusion.refs_1_, bf16[8,256,256]{2,1,0:T(8,128)(2,1)S(1)} %all-to-all-done.1.refs_2_, bf16[8,256,512]{2,1,0:T(8,128)(2,1)S(1)} %copy-done.1, bf16[8,256,512]{2,1,0:T(8,128)(2,1)} %collective-permute-done.14.refs_4_, ...), custom_call_target="tpu_custom_call" | custom-call | tf_op jit(solution)/shard_map/pallas_call | solution.py:109
  169.4 0.4 multiply_reduce_fusion
  170.1 1.6 convolution_convert_fusion
  171.7 97.0 %all_to_all.20 = bf16[8,128,2048]{2,1,0:T(8,128)(2,1)S(1)} all-to-all(bf16[8,128,2048]{2,1,0:T(8,128)(2,1)S(1)} %bitcast.87), channel_id=1, replica_groups=mesh['sp'=8,'dp'=4] {'sp'}, dimensions={0} | all-to-all | bytes 8388608 | tf_op jit(solution)/shard_map/all_to_all | solution.py:266
  268.7 4.5 %fusion.2 = f32[1024,1024]{1,0:T(8,128)S(1)} fusion(bf16[1024,2048]{1,0:T(8,128)(2,1)S(1)} %bitcast.85, bf16[1,2048,1024]{2,1,0:T(8,128)(2,1)S(1)} %copy-done.18), kind=kOutput, calls=%fused_computation.3 | convolution fusion | flops 4294967296 | bytes 12582912 | tf_op jit(solution)/shard_map/dot_general | solution.py:272
  273.2 5.4 %multiply_convert_fusion = bf16[1024,1024]{1,0:T(8,128)(2,1)S(1)} fusion(f32[1024,1024]{1,0:T(8,128)S(1)} %fusion.2, bf16[1024,2048]{1,0:T(8,128)(2,1)S(1)} %bitcast.86, bf16[1,2048,1024]{2,1,0:T(8,128)(2,1)S(1)} %copy-done.19), kind=kOutput, calls=%fused_computation.7 | convolution fusion | flops 4301258752 | bytes 14680064 | tf_op jit(solution)/shard_map/dot_general | solution.py:271
  278.6 6.1 %fusion.6 = bf16[1024,2048]{1,0:T(8,128)(2,1)} fusion(bf16[1024,1024]{1,0:T(8,128)(2,1)S(1)} %multiply_convert_fusion, bf16[1,1024,2048]{2,1,0:T(8,128)(2,1)S(1)} %copy-done.20), kind=kOutput, calls=%fused_computation.9 | convolution fusion | flops 4297064448 | bytes 10485760 | tf_op jit(solution)/shard_map/dot_general | solution.py:274
  284.7 5.0 %all-to-all-start.3 = ((bf16[8,128,2048]{2,1,0:T(8,128)(2,1)}), bf16[8,128,2048]{2,1,0:T(8,128)(2,1)}, u32[]{:S(2)}, u32[]{:S(2)}) async-start(bf16[8,128,2048]{2,1,0:T(8,128)(2,1)} %bitcast.84), calls=%async_computation.3 | async-start | bytes 8388608 | tf_op jit(solution)/shard_map/all_to_all | solution.py:277
  289.7 91.9 %all-to-all-done.3 = bf16[8,128,2048]{2,1,0:T(8,128)(2,1)} async-done(((bf16[8,128,2048]{2,1,0:T(8,128)(2,1)}), bf16[8,128,2048]{2,1,0:T(8,128)(2,1)}, u32[]{:S(2)}, u32[]{:S(2)}) %all-to-all-start.3) | async-done | bytes 4194336 | tf_op jit(solution)/shard_map/all_to_all | solution.py:277
  381.6 3.5 convolution_multiply_fusion
  385.1 4.7 %fusion.14 = bf16[1,256,2048]{2,1,0:T(8,128)(2,1)} fusion(f32[256,2048]{1,0:T(8,128)S(1)} %convolution_multiply_fusion, bf16[1024,2048]{1,0:T(8,128)(2,1)} %bitcast.35, bf16[256,2048]{1,0:T(8,128)(2,1)S(1)} %shard_map.173, bf16[1,256,2048]{2,1,0:T(8,128)(2,1)S(1)} %copy-done.5, f32[256]{0:T(256)S(1)} %bitcast.90, s32[256]{0:T(256)S(1)} %get-tuple-element.5), kind=kOutput, calls=%fused_computation.15 | convolution fusion | flops 1077673984 | bytes 9439232 | tf_op jit(solution)/shard_map/dot_general | solution.py:281
  (95 shorter events, 3.3 us)
Async XLA Ops:
  0.0 15.5 %collective-permute-start.7 = (bf16[256,512]{1,0:T(8,128)(2,1)}, bf16[256,512]{1,0:T(8,128)(2,1)}, u32[]{:S(2)}, u32[]{:S(2)}) collective-permute-start(bf16[256,512]{1,0:T(8,128)(2,1)} %param.26), channel_id=1, source_target_pairs={{0,8},{8,16},{16,24},{24,28},{28,20},{20,12},{12,4},{4,0},{1,9},{9... | collective-permute-start | bytes 786440 | tf_op jit(solution)/shard_map/ppermute | solution.py:65
  3.1 15.5 %collective-permute-start.8 = (bf16[256,512]{1,0:T(8,128)(2,1)}, bf16[256,512]{1,0:T(8,128)(2,1)S(1)}, u32[]{:S(2)}, u32[]{:S(2)}) collective-permute-start(bf16[256,512]{1,0:T(8,128)(2,1)} %param.26), channel_id=1, source_target_pairs={{8,0},{16,8},{24,16},{28,24},{20,28},{12,20},{4,12},{0,4},{9,1},{1... | collective-permute-start | bytes 786440 | tf_op jit(solution)/shard_map/ppermute | solution.py:69
  5.9 1.2 copy-start.4
  9.0 6.4 %copy-start.8 = (bf16[256,512]{1,0:T(8,128)(2,1)S(1)}, bf16[256,512]{1,0:T(8,128)(2,1)}, u32[]{:S(2)}) copy-start(bf16[256,512]{1,0:T(8,128)(2,1)} %param.26) | copy-start | bytes 786436
  9.0 108.6 %all-to-all-start = ((bf16[8,256,384]{2,1,0:T(8,128)(2,1)}), bf16[8,256,384]{2,1,0:T(8,128)(2,1)}, u32[]{:S(2)}, u32[]{:S(2)}) async-start(bf16[8,256,384]{2,1,0:T(8,128)(2,1)} %maximum_bitcast_fusion), calls=%async_computation | async-start | bytes 3145728 | tf_op jit(solution)/shard_map/all_to_all | solution.py:235
  15.4 56.2 %copy-start.7 = (bf16[1,256,256]{2,1,0:T(8,128)(2,1)S(1)}, bf16[1,256,256]{2,1,0:T(8,128)(2,1)}, u32[]{:S(2)}) copy-start(bf16[1,256,256]{2,1,0:T(8,128)(2,1)} %param.20) | copy-start | bytes 393220
  15.4 56.3 %copy-start.17 = (f32[256]{0:T(256)S(1)}, f32[256]{0:T(256)}, u32[]{:S(2)}) copy-start(f32[256]{0:T(256)} %param.23) | copy-start | bytes 3076
  15.5 30.6 %collective-permute-start.9 = (bf16[256,512]{1,0:T(8,128)(2,1)}, bf16[256,512]{1,0:T(8,128)(2,1)S(1)}, u32[]{:S(2)}, u32[]{:S(2)}) collective-permute-start(bf16[256,512]{1,0:T(8,128)(2,1)} %collective-permute-done.7), channel_id=1, source_target_pairs={{0,8},{8,16},{16,24},{24,28},{28,20},{20,12},{12,4},{4,0},{1,9},{9... | collective-permute-start | bytes 786440 | tf_op jit(solution)/shard_map/ppermute | solution.py:65
  18.5 67.5 %copy-start.23 = (s32[8]{0:T(128)S(1)}, s32[8]{0:T(128)}, u32[]{:S(2)}) copy-start(s32[8]{0:T(128)} %constant.85.clone) | copy-start | bytes 100
  18.6 97.2 %copy-start.22 = (s32[8]{0:T(128)S(1)}, s32[8]{0:T(128)}, u32[]{:S(2)}) copy-start(s32[8]{0:T(128)} %constant.87.clone) | copy-start | bytes 100
  18.6 97.9 %copy-start.3 = (s32[8]{0:T(128)S(1)}, s32[8]{0:T(128)}, u32[]{:S(2)}) copy-start(s32[8]{0:T(128)} %constant.86.clone) | copy-start | bytes 100
  18.6 37.5 %collective-permute-start.10 = (bf16[256,512]{1,0:T(8,128)(2,1)S(1)}, bf16[256,512]{1,0:T(8,128)(2,1)S(1)}, u32[]{:S(2)}, u32[]{:S(2)}) collective-permute-start(bf16[256,512]{1,0:T(8,128)(2,1)S(1)} %collective-permute-done.8), channel_id=1, source_target_pairs={{8,0},{16,8},{24,16},{28,24},{20,28},{12,20},{4,12},{0,4},{9,1},{1... | collective-permute-start | bytes 786440 | tf_op jit(solution)/shard_map/ppermute | solution.py:69
  46.1 15.7 %collective-permute-start.11 = (bf16[256,512]{1,0:T(8,128)(2,1)S(1)}, bf16[256,512]{1,0:T(8,128)(2,1)S(1)}, u32[]{:S(2)}, u32[]{:S(2)}) collective-permute-start(bf16[256,512]{1,0:T(8,128)(2,1)S(1)} %collective-permute-done.9), channel_id=1, source_target_pairs={{0,8},{8,16},{16,24},{24,28},{28,20},{20,12},{12,4},{4,0},{1,9},{9... | collective-permute-start | bytes 786440 | tf_op jit(solution)/shard_map/ppermute | solution.py:65
  56.1 8.6 %collective-permute-start.12 = (bf16[256,512]{1,0:T(8,128)(2,1)S(1)}, bf16[256,512]{1,0:T(8,128)(2,1)S(1)}, u32[]{:S(2)}, u32[]{:S(2)}) collective-permute-start(bf16[256,512]{1,0:T(8,128)(2,1)S(1)} %collective-permute-done.10), channel_id=1, source_target_pairs={{8,0},{16,8},{24,16},{28,24},{20,28},{12,20},{4,12},{0,4},{9,1},{1... | collective-permute-start | bytes 786440 | tf_op jit(solution)/shard_map/ppermute | solution.py:69
  61.8 8.2 %collective-permute-start.13 = (bf16[256,512]{1,0:T(8,128)(2,1)S(1)}, bf16[256,512]{1,0:T(8,128)(2,1)S(1)}, u32[]{:S(2)}, u32[]{:S(2)}) collective-permute-start(bf16[256,512]{1,0:T(8,128)(2,1)S(1)} %collective-permute-done.11), channel_id=1, source_target_pairs={{0,8},{8,16},{16,24},{24,28},{28,20},{20,12},{12,4},{4,0},{1,9},{9... | collective-permute-start | bytes 786440 | tf_op jit(solution)/shard_map/ppermute | solution.py:65
  70.1 60.6 %copy-start = (bf16[8,256,512]{2,1,0:T(8,128)(2,1)}, bf16[8,256,512]{2,1,0:T(8,128)(2,1)S(1)}, u32[]{:S(2)}) copy-start(bf16[8,256,512]{2,1,0:T(8,128)(2,1)S(1)} %bitcast_dynamic-update-slice_fusion.refs_3_) | copy-start | bytes 6291460
  70.1 45.7 %collective-permute-start.14 = (bf16[8,256,512]{2,1,0:T(8,128)(2,1)S(1)}, bf16[8,256,512]{2,1,0:T(8,128)(2,1)}, u32[]{:S(2)}, u32[]{:S(2)}) collective-permute-start(bf16[8,256,512]{2,1,0:T(8,128)(2,1)S(1)} %bitcast_dynamic-update-slice_fusion.refs_3_), channel_id=1, source_target_pairs={{0,2},{1,3},{2,0},{3,1},{4,6},{5,7},{6,4},{7,5},{8,10},{9,11},{10,... | collective-permute-start | bytes 6291464 | tf_op jit(solution)/shard_map/ppermute | solution.py:85
  72.0 45.6 %copy-start.6 = (bf16[256,320]{1,0:T(8,128)(2,1)}, bf16[256,320]{1,0:T(8,128)(2,1)S(1)}, u32[]{:S(2)}) copy-start(bf16[256,320]{1,0:T(8,128)(2,1)S(1)} %pad_maximum_fusion.1.refs_4_) | copy-start | bytes 491524
  72.0 6.2 %collective-permute-start = (bf16[256,320]{1,0:T(8,128)(2,1)S(1)}, bf16[256,320]{1,0:T(8,128)(2,1)S(1)}, u32[]{:S(2)}, u32[]{:S(2)}) collective-permute-start(bf16[256,320]{1,0:T(8,128)(2,1)S(1)} %pad_maximum_fusion.1.refs_4_), channel_id=1, source_target_pairs={{0,8},{8,16},{16,24},{24,28},{28,20},{20,12},{12,4},{4,0},{1,9},{9... | collective-permute-start | bytes 491528 | tf_op jit(solution)/shard_map/ppermute | solution.py:65
  73.7 6.1 %collective-permute-start.1 = (bf16[256,320]{1,0:T(8,128)(2,1)S(1)}, bf16[256,320]{1,0:T(8,128)(2,1)S(1)}, u32[]{:S(2)}, u32[]{:S(2)}) collective-permute-start(bf16[256,320]{1,0:T(8,128)(2,1)S(1)} %pad_maximum_fusion.1.refs_4_), channel_id=1, source_target_pairs={{8,0},{16,8},{24,16},{28,24},{20,28},{12,20},{4,12},{0,4},{9,1},{1... | collective-permute-start | bytes 491528 | tf_op jit(solution)/shard_map/ppermute | solution.py:69
  78.2 39.4 %copy-start.9 = (bf16[256,320]{1,0:T(8,128)(2,1)}, bf16[256,320]{1,0:T(8,128)(2,1)S(1)}, u32[]{:S(2)}) copy-start(bf16[256,320]{1,0:T(8,128)(2,1)S(1)} %collective-permute-done.refs_5_) | copy-start | bytes 491524
  78.2 6.9 %collective-permute-start.2 = (bf16[256,320]{1,0:T(8,128)(2,1)S(1)}, bf16[256,320]{1,0:T(8,128)(2,1)S(1)}, u32[]{:S(2)}, u32[]{:S(2)}) collective-permute-start(bf16[256,320]{1,0:T(8,128)(2,1)S(1)} %collective-permute-done.refs_5_), channel_id=1, source_target_pairs={{0,8},{8,16},{16,24},{24,28},{28,20},{20,12},{12,4},{4,0},{1,9},{9... | collective-permute-start | bytes 491528 | tf_op jit(solution)/shard_map/ppermute | solution.py:65
  79.8 37.8 %copy-start.10 = (bf16[256,320]{1,0:T(8,128)(2,1)}, bf16[256,320]{1,0:T(8,128)(2,1)S(1)}, u32[]{:S(2)}) copy-start(bf16[256,320]{1,0:T(8,128)(2,1)S(1)} %collective-permute-done.1.refs_6_) | copy-start | bytes 491524
  79.8 6.8 %collective-permute-start.3 = (bf16[256,320]{1,0:T(8,128)(2,1)S(1)}, bf16[256,320]{1,0:T(8,128)(2,1)S(1)}, u32[]{:S(2)}, u32[]{:S(2)}) collective-permute-start(bf16[256,320]{1,0:T(8,128)(2,1)S(1)} %collective-permute-done.1.refs_6_), channel_id=1, source_target_pairs={{8,0},{16,8},{24,16},{28,24},{20,28},{12,20},{4,12},{0,4},{9,1},{1... | collective-permute-start | bytes 491528 | tf_op jit(solution)/shard_map/ppermute | solution.py:69
  85.1 32.6 %copy-start.11 = (bf16[256,320]{1,0:T(8,128)(2,1)}, bf16[256,320]{1,0:T(8,128)(2,1)S(1)}, u32[]{:S(2)}) copy-start(bf16[256,320]{1,0:T(8,128)(2,1)S(1)} %collective-permute-done.2.refs_7_) | copy-start | bytes 491524
  85.1 7.9 %collective-permute-start.4 = (bf16[256,320]{1,0:T(8,128)(2,1)S(1)}, bf16[256,320]{1,0:T(8,128)(2,1)S(1)}, u32[]{:S(2)}, u32[]{:S(2)}) collective-permute-start(bf16[256,320]{1,0:T(8,128)(2,1)S(1)} %collective-permute-done.2.refs_7_), channel_id=1, source_target_pairs={{0,8},{8,16},{16,24},{24,28},{28,20},{20,12},{12,4},{4,0},{1,9},{9... | collective-permute-start | bytes 491528 | tf_op jit(solution)/shard_map/ppermute | solution.py:65
  86.6 31.0 %copy-start.12 = (bf16[256,320]{1,0:T(8,128)(2,1)}, bf16[256,320]{1,0:T(8,128)(2,1)S(1)}, u32[]{:S(2)}) copy-start(bf16[256,320]{1,0:T(8,128)(2,1)S(1)} %collective-permute-done.3.refs_8_) | copy-start | bytes 491524
  86.6 31.0 %collective-permute-start.5 = (bf16[256,320]{1,0:T(8,128)(2,1)S(1)}, bf16[256,320]{1,0:T(8,128)(2,1)S(1)}, u32[]{:S(2)}, u32[]{:S(2)}) collective-permute-start(bf16[256,320]{1,0:T(8,128)(2,1)S(1)} %collective-permute-done.3.refs_8_), channel_id=1, source_target_pairs={{8,0},{16,8},{24,16},{28,24},{20,28},{12,20},{4,12},{0,4},{9,1},{1... | collective-permute-start | bytes 491528 | tf_op jit(solution)/shard_map/ppermute | solution.py:69
  93.0 24.7 %copy-start.13 = (bf16[256,320]{1,0:T(8,128)(2,1)}, bf16[256,320]{1,0:T(8,128)(2,1)S(1)}, u32[]{:S(2)}) copy-start(bf16[256,320]{1,0:T(8,128)(2,1)S(1)} %collective-permute-done.4.refs_9_) | copy-start | bytes 491524
  93.0 24.6 %collective-permute-start.6 = (bf16[256,320]{1,0:T(8,128)(2,1)S(1)}, bf16[256,320]{1,0:T(8,128)(2,1)}, u32[]{:S(2)}, u32[]{:S(2)}) collective-permute-start(bf16[256,320]{1,0:T(8,128)(2,1)S(1)} %collective-permute-done.4.refs_9_), channel_id=1, source_target_pairs={{0,8},{8,16},{16,24},{24,28},{28,20},{20,12},{12,4},{4,0},{1,9},{9... | collective-permute-start | bytes 491528 | tf_op jit(solution)/shard_map/ppermute | solution.py:65
  93.3 45.2 %collective-permute-start.15 = (bf16[8,256,512]{2,1,0:T(8,128)(2,1)S(1)}, bf16[8,256,512]{2,1,0:T(8,128)(2,1)}, u32[]{:S(2)}, u32[]{:S(2)}) collective-permute-start(bf16[8,256,512]{2,1,0:T(8,128)(2,1)S(1)} %bitcast_dynamic-update-slice_fusion.refs_3_), channel_id=1, source_target_pairs={{0,1},{1,0},{2,3},{3,2},{4,5},{5,4},{6,7},{7,6},{8,9},{9,8},{10,11... | collective-permute-start | bytes 6291464 | tf_op jit(solution)/shard_map/ppermute | solution.py:89
  115.7 46.7 %collective-permute-start.16 = (bf16[8,256,512]{2,1,0:T(8,128)(2,1)}, bf16[8,256,512]{2,1,0:T(8,128)(2,1)}, u32[]{:S(2)}, u32[]{:S(2)}) collective-permute-start(bf16[8,256,512]{2,1,0:T(8,128)(2,1)} %collective-permute-done.14.refs_4_), channel_id=1, source_target_pairs={{0,1},{1,0},{2,3},{3,2},{4,5},{5,4},{6,7},{7,6},{8,9},{9,8},{10,11... | collective-permute-start | bytes 6291464 | tf_op jit(solution)/shard_map/ppermute | solution.py:89
  117.6 0.7 copy-start.14
  130.7 5.4 %copy-start.15 = (s32[1,256,2]{1,2,0:T(2,128)S(1)}, s32[1,256,2]{1,2,0:T(2,128)}, u32[]{:S(2)}) copy-start(s32[1,256,2]{1,2,0:T(2,128)} %param.31) | copy-start | bytes 6148
  130.7 31.8 %copy-start.2 = (s32[8]{0:T(128)S(1)}, s32[8]{0:T(128)}, u32[]{:S(2)}) copy-start(s32[8]{0:T(128)} %gather_fusion) | copy-start | bytes 100
  130.7 31.8 %all-to-all-start.1 = ((bf16[8,256,256]{2,1,0:T(8,128)(2,1)}), bf16[8,256,256]{2,1,0:T(8,128)(2,1)S(1)}, u32[]{:S(2)}, u32[]{:S(2)}) async-start(bf16[8,256,256]{2,1,0:T(8,128)(2,1)} %bitcast.83), calls=%async_computation.1 | async-start | bytes 2097152 | tf_op jit(solution)/shard_map/all_to_all | solution.py:248
  162.5 1.6 copy-start.1
  164.1 5.3 %copy-start.5 = (bf16[1,256,2048]{2,1,0:T(8,128)(2,1)S(1)}, bf16[1,256,2048]{2,1,0:T(8,128)(2,1)}, u32[]{:S(2)}) copy-start(bf16[1,256,2048]{2,1,0:T(8,128)(2,1)} %param.22) | copy-start | bytes 3145732
  169.4 0.7 copy-start.21
  171.6 97.1 %copy-start.18 = (bf16[1,2048,1024]{2,1,0:T(8,128)(2,1)S(1)}, bf16[1,2048,1024]{2,1,0:T(8,128)(2,1)}, u32[]{:S(2)}) copy-start(bf16[1,2048,1024]{2,1,0:T(8,128)(2,1)} %param.29) | copy-start | bytes 12582916
  268.7 4.5 %copy-start.19 = (bf16[1,2048,1024]{2,1,0:T(8,128)(2,1)S(1)}, bf16[1,2048,1024]{2,1,0:T(8,128)(2,1)}, u32[]{:S(2)}) copy-start(bf16[1,2048,1024]{2,1,0:T(8,128)(2,1)} %param.28) | copy-start | bytes 12582916
  273.2 5.4 %copy-start.20 = (bf16[1,1024,2048]{2,1,0:T(8,128)(2,1)S(1)}, bf16[1,1024,2048]{2,1,0:T(8,128)(2,1)}, u32[]{:S(2)}) copy-start(bf16[1,1024,2048]{2,1,0:T(8,128)(2,1)} %param.30) | copy-start | bytes 12582916
  284.7 5.0 %copy-start.16 = (f32[1,256,2]{1,2,0:T(2,128)S(1)}, f32[1,256,2]{1,2,0:T(2,128)}, u32[]{:S(2)}) copy-start(f32[1,256,2]{1,2,0:T(2,128)} %param.32) | copy-start | bytes 6148
  284.7 96.9 %all-to-all-start.3 = ((bf16[8,128,2048]{2,1,0:T(8,128)(2,1)}), bf16[8,128,2048]{2,1,0:T(8,128)(2,1)}, u32[]{:S(2)}, u32[]{:S(2)}) async-start(bf16[8,128,2048]{2,1,0:T(8,128)(2,1)} %bitcast.84), calls=%async_computation.3 | async-start | bytes 8388608 | tf_op jit(solution)/shard_map/all_to_all | solution.py:277
